TPU v7x, 32 devices: a whole 2x2x4 slice. The times are simulated.
32 devices in a mesh: fs: 4 (over z), rep: 4 (over y, x), tp: 2 (over core).
Axes of the slice: x: 2, y: 2, z: 4, core: 2. Of those that a mesh axis runs over, the one named last changes fastest.
Arguments:
- normed: bfloat16 [10240, 2048], P(('fs', 'rep')), may hold values from -150 to 150
- rec_cot: bfloat16 [10240, 2048], P(('fs', 'rep'), 'tp'), may hold values from -1.4823177 to 1.4823177
- conv_out: bfloat16 [10240, 2048], P(('fs', 'rep'), 'tp'), may hold values from -6 to 6
- gate_cot: bfloat16 [10240, 2048], P(('fs', 'rep'), 'tp'), may hold values from -0.05908203 to 0.05908203
- rec_weight: float32 [2048, 2048], P('fs', 'tp'), may hold values from -0.125 to 0.125
- rec_moment: float32 [2048, 2048], P('fs', 'tp'), may hold values from -6 to 6
- rec_right: bfloat16 [2048, 256], P('tp'), may hold values from -1 to 2
- gate_weight: float32 [8, 256, 256], P('tp', 'fs'), may hold values from -0.375 to 0.375
- gate_moment: float32 [8, 256, 256], P('tp', 'fs'), may hold values from -6 to 6
- gate_left: bfloat16 [8, 256, 256], P('tp', 'fs'), may hold values from -1 to 2
- gate_right: bfloat16 [8, 256, 256], P('tp'), may hold values from -1 to 2
Outputs:
- rec_weight_new: float32 [2048, 2048], P('fs', 'tp')
- rec_moment_new: float32 [2048, 2048], P('fs', 'tp')
- rec_step: float32 [2048, 2048], P('fs', 'tp')
- rec_copy: bfloat16 [2048, 2048], P('fs', 'tp')
- gate_weight_new: float32 [8, 256, 256], P('tp', 'fs')
- gate_moment_new: float32 [8, 256, 256], P('tp', 'fs')
- gate_step: float32 [8, 256, 256], P('tp', 'fs')
- gate_copy: bfloat16 [8, 256, 256], P('tp', 'fs')
All inputs are finite; a program needn't handle non-finite values.
Results may differ from a plain program's by a relative error of at most 0.001.
Values sent between devices are 32-bit elements; how exact they have to be, the bound alone decides.
A program may use at most 64 MiB of HBM per device.

v0:
```python
import jax
import jax.numpy as jnp
from jax import lax
from jax.sharding import PartitionSpec as P

BETA = 0.9
LEARN_RATE = 0.02
EPSILON = 1e-06


def precondition_right(gradient, factor):
    row_count = gradient.shape[0]
    block_size = factor.shape[1]
    blocks = factor.shape[0] // block_size
    shaped = gradient.reshape(row_count, blocks, block_size)
    factors = factor.astype(jnp.float32).reshape(blocks, block_size, block_size)
    result = jnp.einsum("rbi,bij->rbj", shaped, factors, precision=lax.Precision.HIGHEST)
    return result.reshape(row_count, blocks * block_size)


def shards(
    normed,
    rec_cot,
    conv_out,
    gate_cot,
    rec_weight,
    rec_moment,
    rec_right,
    gate_weight,
    gate_moment,
    gate_left,
    gate_right,
):
    token_count = normed.shape[0]
    columns = normed
    partial_rows = lax.psum_scatter(
        lax.dot_general(
            columns, rec_cot, (((0,), (0,)), ((), ())), preferred_element_type=jnp.float32
        ),
        "fs",
        scatter_dimension=0,
        tiled=True,
    )
    rec_grad = lax.psum(partial_rows, "rep")
    rec_pre = precondition_right(rec_grad, rec_right)
    block_count, own_rows, block_size = gate_weight.shape
    conv_blocks = conv_out.reshape(token_count, block_count, block_size)
    cot_blocks = gate_cot.reshape(token_count, block_count, block_size)
    gate_term = jnp.einsum(
        "tbi,tbj->bij", conv_blocks, cot_blocks, preferred_element_type=jnp.float32
    )
    right_factor = gate_right.astype(jnp.float32)
    left_factor = gate_left.astype(jnp.float32)
    part_grad = lax.psum_scatter(gate_term, "fs", scatter_dimension=1, tiled=True)
    gate_grad = lax.psum(part_grad, "rep")
    right_done = jnp.einsum(
        "bij,bjk->bik", gate_grad, right_factor, precision=lax.Precision.HIGHEST
    )
    columns = left_factor
    gate_pre = jnp.einsum(
        "bri,bik->brk",
        columns,
        lax.all_gather(right_done, "fs", axis=1, tiled=True),
        precision=lax.Precision.HIGHEST,
    )
    rec_moment_new = BETA * rec_moment + rec_pre
    gate_moment_new = BETA * gate_moment + gate_pre
    totals = lax.psum(
        (
            jnp.sum(rec_grad * rec_grad),
            jnp.sum(rec_moment_new * rec_moment_new),
            jnp.sum(gate_grad * gate_grad),
            jnp.sum(gate_moment_new * gate_moment_new),
        ),
        ("fs", "tp"),
    )
    rec_scale = jnp.sqrt(totals[0]) / jnp.sqrt(totals[1] + EPSILON)
    gate_scale = jnp.sqrt(totals[2]) / jnp.sqrt(totals[3] + EPSILON)
    rec_taken = LEARN_RATE * rec_scale * rec_moment_new
    gate_taken = LEARN_RATE * gate_scale * gate_moment_new
    rec_new = rec_weight - rec_taken
    gate_new = gate_weight - gate_taken
    return (
        rec_new,
        rec_moment_new,
        rec_taken,
        rec_new.astype(jnp.bfloat16),
        gate_new,
        gate_moment_new,
        gate_taken,
        gate_new.astype(jnp.bfloat16),
    )


def solution(mesh):
    in_specs = (
        P(("fs", "rep"), None),
        P(("fs", "rep"), "tp"),
        P(("fs", "rep"), "tp"),
        P(("fs", "rep"), "tp"),
        P("fs", "tp"),
        P("fs", "tp"),
        P("tp", None),
        P("tp", "fs", None),
        P("tp", "fs", None),
        P("tp", "fs", None),
        P("tp", None, None),
    )
    out_specs = (
        P("fs", "tp"),
        P("fs", "tp"),
        P("fs", "tp"),
        P("fs", "tp"),
        P("tp", "fs", None),
        P("tp", "fs", None),
        P("tp", "fs", None),
        P("tp", "fs", None),
    )
    return jax.shard_map(shards, mesh=mesh, in_specs=in_specs, out_specs=out_specs, check_vma=False)
```

profile of v0, /device:TPU:0, one launch (start us, length us, event | category | flops | bytes accessed | tf_op | source)
XLA Modules:
  0.0 330.2 jit_solution(16885048392378607039)
XLA Ops:
  7.2 0.0 copy-start
  7.2 0.0 reduce-scatter.5.cloned.1.call-start
  7.2 2.6 copy.25
  9.8 3.3 fusion.3
  13.1 0.0 reduce-scatter.5.cloned.1.call-update
  13.1 0.0 reduce-scatter.3.cloned.1.call-start
  13.1 0.0 copy-done
  13.1 7.0 %fusion.9 = f32[2048,1024]{1,0:T(8,128)} fusion(bf16[640,2048]{1,0:T(8,128)(2,1)S(1)} %copy-done, bf16[640,1024]{1,0:T(8,128)(2,1)} %param.12), kind=kOutput, calls=%fused_computation.17 | convolution fusion | flops 2684354560 | bytes 12320768 | tf_op jit(solution)/shard_map/dot_general | solution.py:37
  20.1 0.0 reduce-scatter.3.cloned.1.call-update
  20.2 0.0 copy-start.3
  20.2 0.0 all-reduce.4.cloned.1.call-start
  20.2 23.0 %reduce-scatter.5.cloned.1.call-done = f32[4,64,256]{2,1,0:T(8,128)} async-done(((f32[4,256,256]{2,1,0:T(8,128)}), f32[4,64,256]{2,1,0:T(8,128)}) %reduce-scatter.5.cloned.1.call-update) | async-done | bytes 262160 | tf_op jit(solution)/shard_map/reduce_scatter | solution.py:54
  43.2 145.5 %reduce-scatter.3.cloned.1.call-done = f32[512,1024]{1,0:T(8,128)} async-done(((f32[2048,1024]{1,0:T(8,128)}), f32[512,1024]{1,0:T(8,128)}) %reduce-scatter.3.cloned.1.call-update) | async-done | bytes 2097168 | tf_op jit(solution)/shard_map/reduce_scatter | solution.py:36
  188.8 0.0 all-reduce.4.cloned.1.call-update
  188.8 0.0 all-gather.2.cloned.1.call-start
  188.8 77.6 %all-reduce.4.cloned.1.call-done = (f32[512,1024]{1,0:T(8,128)}, f32[4,64,256]{2,1,0:T(8,128)}) async-done(((f32[512,1024]{1,0:T(8,128)}, f32[4,64,256]{2,1,0:T(8,128)}), (f32[512,1024]{1,0:T(8,128)}, f32[4,64,256]{2,1,0:T(8,128)})) %all-reduce.4.cloned.1.call-update) | async-done | bytes 2359312 | tf_op jit(solution)/shard_map/psum | solution.py:44
  266.5 2.2 fusion.10
  268.7 0.0 all-gather.2.cloned.1.call-update
  268.7 0.0 copy-done.3
  268.7 4.1 %fusion = f32[4,512,256]{1,2,0:T(8,128)} fusion(bf16[4,256,256]{2,1,0:T(8,128)(2,1)S(1)} %bitcast.29, f32[64,4,8,256]{3,2,1,0:T(8,128)} %bitcast.25), kind=kOutput, calls=%fused_computation | convolution fusion | flops 1610612736 | bytes 4718592 | tf_op jit(solution)/shard_map/rbi,bij->rbj/dot_general | solution.py:17
  272.8 2.9 copy.21
  275.8 0.0 copy-done.2
  275.8 0.7 multiply_reduce_fusion.3
  276.4 5.7 %multiply_reduce_fusion = (f32[]{:T(128)}, f32[512,1024]{1,0:T(8,128)}, f32[]{:T(128)}) fusion(f32[512,1024]{1,0:T(8,128)} %copy.21, f32[512,1024]{1,0:T(8,128)} %param.16, f32[512,1024]{1,0:T(8,128)} %get-tuple-element.12), kind=kLoop, calls=%fused_computation.3 | loop fusion | flops 3145726 | bytes 8388616 | tf_op jit(solution)/shard_map/reduce_sum | solution.py:71
  282.1 14.7 %all-gather.2.cloned.1.call-done = f32[4,256,256]{2,1,0:T(8,128)} async-done(((f32[4,64,256]{2,1,0:T(8,128)}), f32[4,256,256]{2,1,0:T(8,128)}) %all-gather.2.cloned.1.call-update) | async-done | bytes 1048592 | tf_op jit(solution)/shard_map/all_gather | solution.py:63
  296.8 0.0 copy-done.4
  296.8 0.0 copy-done.6
  296.8 2.4 multiply_reduce_fusion.2
  299.2 15.3 %all-reduce = (f32[]{:T(128)}, f32[]{:T(128)}, f32[]{:T(128)}, f32[]{:T(128)}) all-reduce(f32[]{:T(128)} %get-tuple-element.24, f32[]{:T(128)} %get-tuple-element.20, f32[]{:T(128)} %multiply_reduce_fusion.3, f32[]{:T(128)} %get-tuple-element.22), channel_id=1, replica_groups=mesh['fs'=4,'rep'=4,'tp'=2] {'fs','tp'}, use_global_device_ids=true, to_apply=%region_3.0 | all-reduce | flops 4 | bytes 32 | tf_op jit(solution)/shard_map/psum | solution.py:68
  317.3 0.0 copy-start.5
  317.3 5.5 %fusion.8 = (bf16[512,1024]{1,0:T(8,128)(2,1)}, f32[512,1024]{1,0:T(8,128)}, f32[512,1024]{1,0:T(8,128)}) fusion(f32[512,1024]{1,0:T(8,128)} %param.15, f32[512,1024]{1,0:T(8,128)} %get-tuple-element.21, f32[]{:T(128)S(6)} %mul.46), kind=kLoop, calls=%fused_computation.16 | loop fusion | flops 1572864 | bytes 9437188 | tf_op jit(solution)/shard_map/convert_element_type | solution.py:87
  322.8 0.9 fusion.7
  (6 shorter events, 0.0 us)
Async XLA Ops:
  7.2 6.0 %copy-start = (bf16[640,2048]{1,0:T(8,128)(2,1)S(1)}, bf16[640,2048]{1,0:T(8,128)(2,1)}, u32[]{:S(2)}) copy-start(bf16[640,2048]{1,0:T(8,128)(2,1)} %param.11) | copy-start | bytes 7864324
  7.2 36.1 %reduce-scatter.5.cloned.1.call-start = ((), (), s32[]{:S(2)}) async-start(), calls=%async_computation.3 | async-start | bytes 1310720 | tf_op jit(solution)/shard_map/reduce_scatter | solution.py:54
  13.1 175.7 %reduce-scatter.3.cloned.1.call-start = ((), (), s32[]{:S(2)}) async-start(), calls=%async_computation.2 | async-start | bytes 10485760 | tf_op jit(solution)/shard_map/reduce_scatter | solution.py:36
  20.2 248.5 %copy-start.3 = (bf16[1024,256]{1,0:T(8,128)(2,1)S(1)}, bf16[1024,256]{1,0:T(8,128)(2,1)}, u32[]{:S(2)}) copy-start(bf16[1024,256]{1,0:T(8,128)(2,1)} %param.17) | copy-start | bytes 1572868
  20.2 246.3 %all-reduce.4.cloned.1.call-start = ((), (), s32[]{:S(2)}) async-start(), calls=%async_computation.5 | async-start | bytes 4718592 | tf_op jit(solution)/shard_map/psum | solution.py:44
  188.8 108.1 %all-gather.2.cloned.1.call-start = ((), (), s32[]{:S(2)}) async-start(), calls=%async_computation.4 | async-start | bytes 1310720 | tf_op jit(solution)/shard_map/all_gather | solution.py:63
  272.8 2.9 copy-start.2
  276.4 20.4 %copy-start.4 = (f32[4,64,256]{2,1,0:T(8,128)S(1)}, f32[4,64,256]{2,1,0:T(8,128)}, u32[]{:S(2)}) copy-start(f32[4,64,256]{2,1,0:T(8,128)} %param.19) | copy-start | bytes 786436
  276.4 20.4 %copy-start.6 = (bf16[4,64,256]{2,1,0:T(8,128)(2,1)S(1)}, bf16[4,64,256]{2,1,0:T(8,128)(2,1)}, u32[]{:S(2)}) copy-start(bf16[4,64,256]{2,1,0:T(8,128)(2,1)} %param.20) | copy-start | bytes 393220
  299.2 23.6 %copy-start.1 = (f32[4,64,256]{2,1,0:T(8,128)}, f32[4,64,256]{2,1,0:T(8,128)S(1)}, u32[]{:S(2)}) copy-start(f32[4,64,256]{2,1,0:T(8,128)S(1)} %get-tuple-element.23) | copy-start | bytes 786436
  317.3 5.5 %copy-start.5 = (f32[4,64,256]{2,1,0:T(8,128)S(1)}, f32[4,64,256]{2,1,0:T(8,128)}, u32[]{:S(2)}) copy-start(f32[4,64,256]{2,1,0:T(8,128)} %param.18) | copy-start | bytes 786436
Sparse Core Ops, SparseCore 0:
  13.2 29.9 reduce-scatter.4
  45.6 143.1 reduce-scatter.2
  191.9 74.4 all-reduce.3
  268.8 27.9 all-gather.1
where the time goes:
time: 331 us; the launch traced here: 330 us
  waiting for transfers between devices  261 us (79%)
  matrix products  19 us (6%)
  between operations  16.6 us (5%)
  blocking collectives  15.3 us (5%)
  other arithmetic  12.7 us (4%)
  local copies, waits for them, and re-layouts  5.54 us (2%)
    reduce_scatter x1, waiting for transfers between devices, shards(): lax.psum_scatter(lax.dot_general(columns, rec_cot, (((0,), (0,)), ((), ()...  146 us
    psum x1, waiting for transfers between devices, shards(): rec_grad = lax.psum(partial_rows, 'rep')  77.6 us
    reduce_scatter x1, waiting for transfers between devices, shards(): lax.psum_scatter(gate_term, 'fs', scatter_dimension=1, tiled=True)  23 us
    psum x1, blocking collectives, shards(): lax.psum((jnp.sum(rec_grad * rec_grad), jnp.sum(rec_moment_new * rec_mome...  15.3 us
    all_gather x1, waiting for transfers between devices, shards(): lax.all_gather(right_done, 'fs', axis=1, tiled=True)  14.7 us
    dot_general x1, matrix products, shards(): lax.dot_general(columns, rec_cot, (((0,), (0,)), ((), ())), preferred_ele...  7 us
  transfers between devices with their start and end apart: 4, of which 4 were waited for; matrix products, arithmetic and copies ran while one was open for 6% of the time, Pallas kernels for 0%

commit v1 on v0

--- a/solution.py
+++ b/solution.py
@@ -41,7 +41,7 @@
         scatter_dimension=0,
         tiled=True,
     )
-    rec_grad = lax.psum(partial_rows, "rep")
+    rec_grad = jnp.sum(lax.all_gather(partial_rows, "rep"), axis=0)
     rec_pre = precondition_right(rec_grad, rec_right)
     block_count, own_rows, block_size = gate_weight.shape
     conv_blocks = conv_out.reshape(token_count, block_count, block_size)

time: 331 us -> 408 us (1.23)
  waiting for transfers between devices: 261 us -> 328 us
  other arithmetic: 12.7 us -> 18.5 us
    all_gather x0 -> x1, waiting for transfers between devices: none -> 86.2 us  [shards(): rec_grad = jnp.sum(lax.all_gather(partial_rows, 'rep'), axis=0)]
    psum x1, waiting for transfers between devices: 77.6 us -> 37.4 us  [shards(): gate_grad = lax.psum(part_grad, 'rep')]
    all_gather x1, waiting for transfers between devices: 14.7 us -> 29.9 us  [shards(): lax.all_gather(right_done, 'fs', axis=1, tiled=True)]
    reduce_scatter x1, waiting for transfers between devices: 23 us -> 30.1 us  [shards(): lax.psum_scatter(gate_term, 'fs', scatter_dimension=1, tiled=True)]
    reduce_sum x0 -> x1, other arithmetic: none -> 5.88 us  [shards(): rec_grad = jnp.sum(lax.all_gather(partial_rows, 'rep'), axis=0)]
  transfers between devices with their start and end apart: 4 -> 5, of which waited for: 4 -> 5; matrix products, arithmetic and copies ran while one was open for 6% -> 3% of each run, Pallas kernels for 0% -> 0%
where the time goes in v1:
time: 408 us
  waiting for transfers between devices  328 us (80%)
  matrix products  18.9 us (5%)
  other arithmetic  18.5 us (5%)
  blocking collectives  16.8 us (4%)
  between operations  16.6 us (4%)
  local copies, waits for them, and re-layouts  8.43 us (2%)
    reduce_scatter x1, waiting for transfers between devices, shards(): lax.psum_scatter(lax.dot_general(columns, rec_cot, (((0,), (0,)), ((), ()...  145 us
    all_gather x1, waiting for transfers between devices, shards(): rec_grad = jnp.sum(lax.all_gather(partial_rows, 'rep'), axis=0)  86.2 us
    psum x1, waiting for transfers between devices, shards(): gate_grad = lax.psum(part_grad, 'rep')  37.4 us
    reduce_scatter x1, waiting for transfers between devices, shards(): lax.psum_scatter(gate_term, 'fs', scatter_dimension=1, tiled=True)  30.1 us
    all_gather x1, waiting for transfers between devices, shards(): lax.all_gather(right_done, 'fs', axis=1, tiled=True)  29.9 us
    psum x1, blocking collectives, shards(): lax.psum((jnp.sum(rec_grad * rec_grad), jnp.sum(rec_moment_new * rec_mome...  16.8 us
  transfers between devices with their start and end apart: 5, of which 5 were waited for; matrix products, arithmetic and copies ran while one was open for 3% of the time, Pallas kernels for 0%

profile of v1, /device:TPU:0, one launch (start us, length us, event | category | flops | bytes accessed | tf_op | source)
XLA Modules:
  0.0 407.9 jit_solution(10161963380702721682)
XLA Ops:
  7.2 0.0 copy-start
  7.2 0.0 reduce-scatter.5.cloned.1.call-start
  7.2 2.6 copy.36
  9.8 3.3 fusion
  13.1 0.0 reduce-scatter.5.cloned.1.call-update
  13.1 0.0 all-reduce.3.cloned.1.call-start
  13.1 30.1 %reduce-scatter.5.cloned.1.call-done = f32[4,64,256]{2,1,0:T(8,128)} async-done(((f32[4,256,256]{2,1,0:T(8,128)}), f32[4,64,256]{2,1,0:T(8,128)}) %reduce-scatter.5.cloned.1.call-update) | async-done | bytes 262160 | tf_op jit(solution)/shard_map/reduce_scatter | solution.py:54
  43.2 0.0 all-reduce.3.cloned.1.call-update
  43.3 0.0 reduce-scatter.3.cloned.1.call-start
  43.3 7.0 %fusion.6 = f32[2048,1024]{1,0:T(8,128)} fusion(bf16[640,2048]{1,0:T(8,128)(2,1)S(1)} %copy-done, bf16[640,1024]{1,0:T(8,128)(2,1)} %param.12), kind=kOutput, calls=%fused_computation.14 | convolution fusion | flops 2684354560 | bytes 12320768 | tf_op jit(solution)/shard_map/dot_general | solution.py:37
  50.3 0.0 reduce-scatter.3.cloned.1.call-update
  50.3 0.0 copy-start.6
  50.4 0.0 all-gather.4.cloned.1.call-start
  50.4 37.4 %all-reduce.3.cloned.1.call-done = f32[4,64,256]{2,1,0:T(8,128)} async-done(((f32[4,64,256]{2,1,0:T(8,128)}), f32[4,64,256]{2,1,0:T(8,128)}) %all-reduce.3.cloned.1.call-update) | async-done | bytes 262160 | tf_op jit(solution)/shard_map/psum | solution.py:55
  87.8 2.1 fusion.8
  89.9 0.0 all-gather.4.cloned.1.call-update
  89.9 0.0 all-gather.6.cloned.1.call-start
  90.0 144.8 %reduce-scatter.3.cloned.1.call-done = f32[512,1024]{1,0:T(8,128)} async-done(((f32[2048,1024]{1,0:T(8,128)}), f32[512,1024]{1,0:T(8,128)}) %reduce-scatter.3.cloned.1.call-update) | async-done | bytes 2097168 | tf_op jit(solution)/shard_map/reduce_scatter | solution.py:36
  234.8 0.0 all-gather.6.cloned.1.call-update
  234.8 0.7 multiply_reduce_fusion.3
  235.5 29.9 %all-gather.4.cloned.1.call-done = f32[4,256,256]{2,1,0:T(8,128)} async-done(((f32[4,64,256]{2,1,0:T(8,128)}), f32[4,256,256]{2,1,0:T(8,128)}) %all-gather.4.cloned.1.call-update) | async-done | bytes 1048592 | tf_op jit(solution)/shard_map/all_gather | solution.py:63
  265.4 2.4 multiply_reduce_fusion.2
  267.8 86.2 %all-gather.6.cloned.1.call-done = f32[2048,1024]{1,0:T(8,128)} async-done(((f32[512,1024]{1,0:T(8,128)}), f32[2048,1024]{1,0:T(8,128)}) %all-gather.6.cloned.1.call-update) | async-done | bytes 8388624 | tf_op jit(solution)/shard_map/all_gather | solution.py:44
  354.0 5.9 %reduce_sum.45 = f32[512,1024]{1,0:T(8,128)} reduce(f32[4,512,1024]{2,1,0:T(8,128)} %bitcast.24, f32[]{:T(128)} %constant.4.clone.1), dimensions={0}, to_apply=%region_1.0 | reduce | flops 1572864 | bytes 10485764 | tf_op jit(solution)/shard_map/reduce_sum | solution.py:44
  359.9 2.9 copy.28
  362.8 4.1 %fusion.7 = f32[4,512,256]{1,2,0:T(8,128)} fusion(f32[512,4,256]{0,2,1:T(8,128)} %bitcast.26, bf16[4,256,256]{2,1,0:T(8,128)(2,1)S(1)} %bitcast.29), kind=kOutput, calls=%fused_computation.15 | convolution fusion | flops 1610612736 | bytes 4718592 | tf_op jit(solution)/shard_map/rbi,bij->rbj/dot_general | solution.py:17
  366.9 2.9 copy.31
  369.8 5.6 %multiply_reduce_fusion = (f32[]{:T(128)}, f32[512,1024]{1,0:T(8,128)}, f32[]{:T(128)}) fusion(f32[512,1024]{1,0:T(8,128)} %copy.31, f32[512,1024]{1,0:T(8,128)} %param.16, f32[512,1024]{1,0:T(8,128)} %reduce_sum.45), kind=kLoop, calls=%fused_computation | loop fusion | flops 3145726 | bytes 8388616 | tf_op jit(solution)/shard_map/reduce_sum | solution.py:71
  375.4 16.8 %all-reduce = (f32[]{:T(128)}, f32[]{:T(128)}, f32[]{:T(128)}, f32[]{:T(128)}) all-reduce(f32[]{:T(128)} %get-tuple-element.22, f32[]{:T(128)} %get-tuple-element.18, f32[]{:T(128)} %multiply_reduce_fusion.3, f32[]{:T(128)} %get-tuple-element.20), channel_id=1, replica_groups=mesh['fs'=4,'rep'=4,'tp'=2] {'fs','tp'}, use_global_device_ids=true, to_apply=%region_3.0 | all-reduce | flops 4 | bytes 32 | tf_op jit(solution)/shard_map/psum | solution.py:68
  395.0 0.0 copy-start.5
  395.0 5.5 %fusion.5 = (bf16[512,1024]{1,0:T(8,128)(2,1)}, f32[512,1024]{1,0:T(8,128)}, f32[512,1024]{1,0:T(8,128)}) fusion(f32[512,1024]{1,0:T(8,128)} %param.15, f32[512,1024]{1,0:T(8,128)} %get-tuple-element.19, f32[]{:T(128)S(6)} %mul.46), kind=kLoop, calls=%fused_computation.13 | loop fusion | flops 1572864 | bytes 9437188 | tf_op jit(solution)/shard_map/convert_element_type | solution.py:87
  400.5 0.9 fusion.4
  (11 shorter events, 0.0 us)
Async XLA Ops:
  7.2 36.1 %copy-start = (bf16[640,2048]{1,0:T(8,128)(2,1)S(1)}, bf16[640,2048]{1,0:T(8,128)(2,1)}, u32[]{:S(2)}) copy-start(bf16[640,2048]{1,0:T(8,128)(2,1)} %param.11) | copy-start | bytes 7864324
  7.2 36.1 %reduce-scatter.5.cloned.1.call-start = ((), (), s32[]{:S(2)}) async-start(), calls=%async_computation.3 | async-start | bytes 1310720 | tf_op jit(solution)/shard_map/reduce_scatter | solution.py:54
  13.1 74.7 %all-reduce.3.cloned.1.call-start = ((), (), s32[]{:S(2)}) async-start(), calls=%async_computation.4 | async-start | bytes 524288 | tf_op jit(solution)/shard_map/psum | solution.py:55
  43.3 191.5 %reduce-scatter.3.cloned.1.call-start = ((), (), s32[]{:S(2)}) async-start(), calls=%async_computation.2 | async-start | bytes 10485760 | tf_op jit(solution)/shard_map/reduce_scatter | solution.py:36
  50.3 37.5 %copy-start.4 = (bf16[4,256,256]{2,1,0:T(8,128)(2,1)S(1)}, bf16[4,256,256]{2,1,0:T(8,128)(2,1)}, u32[]{:S(2)}) copy-start(bf16[4,256,256]{2,1,0:T(8,128)(2,1)} %param.21) | copy-start | bytes 1572868
  50.3 215.1 %copy-start.6 = (bf16[4,64,256]{2,1,0:T(8,128)(2,1)S(1)}, bf16[4,64,256]{2,1,0:T(8,128)(2,1)}, u32[]{:S(2)}) copy-start(bf16[4,64,256]{2,1,0:T(8,128)(2,1)} %param.20) | copy-start | bytes 393220
  50.4 215.1 %all-gather.4.cloned.1.call-start = ((), (), s32[]{:S(2)}) async-start(), calls=%async_computation.5 | async-start | bytes 1310720 | tf_op jit(solution)/shard_map/all_gather | solution.py:63
  87.8 147.0 %copy-start.2 = (f32[4,64,256]{2,1,0:T(8,128)S(1)}, f32[4,64,256]{2,1,0:T(8,128)}, u32[]{:S(2)}) copy-start(f32[4,64,256]{2,1,0:T(8,128)} %all-reduce.3.cloned.1.call-done) | copy-start | bytes 786436
  89.9 264.1 %all-gather.6.cloned.1.call-start = ((), (), s32[]{:S(2)}) async-start(), calls=%async_computation.6 | async-start | bytes 10485760 | tf_op jit(solution)/shard_map/all_gather | solution.py:44
  267.8 132.7 %copy-start.1 = (f32[4,64,256]{2,1,0:T(8,128)}, f32[4,64,256]{2,1,0:T(8,128)S(1)}, u32[]{:S(2)}) copy-start(f32[4,64,256]{2,1,0:T(8,128)S(1)} %get-tuple-element.21) | copy-start | bytes 786436
  359.9 2.9 copy-start.3
  395.0 5.5 %copy-start.5 = (f32[4,64,256]{2,1,0:T(8,128)S(1)}, f32[4,64,256]{2,1,0:T(8,128)}, u32[]{:S(2)}) copy-start(f32[4,64,256]{2,1,0:T(8,128)} %param.18) | copy-start | bytes 786436
Sparse Core Ops, SparseCore 0:
  13.2 29.9 reduce-scatter.4
  46.2 41.5 all-reduce.2
  90.1 144.6 reduce-scatter.2
  236.8 28.5 all-gather.3
  267.1 86.8 all-gather.5
